TPU v7x, 32 devices: a whole 2x2x4 slice. The times are simulated.
32 devices in a mesh: sp: 8 (over z, y), tp: 4 (over x, core).
Axes of the slice: x: 2, y: 2, z: 4, core: 2. Of those that a mesh axis runs over, the one named last changes fastest.
Arguments:
- stream: bfloat16 [1536, 2048], P('sp'), may hold values from -6 to 6
- upstream: bfloat16 [1536, 2048], P('sp'), may hold values from -6 to 6
- expert_gain: float32 [2048], replicated, may hold values from 0.1 to 1.9
- expert_ids: int32 [1536, 2], P('sp'), may hold values from 0 to 7, all different within a row; in each aligned block of 192 rows (0 to 191, 192 to 383, ...) at most 60 rows name the same one
- group_weight: float32 [1536], P('sp'), may hold values from 0.25 to 1
- pair_scores: float32 [1536, 2], P('sp'), may hold values from -6 to 6
- gate_weight: bfloat16 [8, 2048, 1024], P('sp', None, 'tp'), may hold values from -0.125 to 0.125
- up_weight: bfloat16 [8, 2048, 1024], P('sp', None, 'tp'), may hold values from -0.125 to 0.125
- down_weight: bfloat16 [8, 1024, 2048], P('sp', 'tp'), may hold values from -0.1875 to 0.1875
- mixer_weight: bfloat16 [1024, 2048], P('tp'), may hold values from -0.1875 to 0.1875
- filtered: bfloat16 [1536, 1024], P('sp', 'tp'), may hold values from -1000 to 1000
- channel_gain: float32 [1024], P('tp'), may hold values from 0.1 to 1.9
- kernel_taps: float32 [31, 1024], P(None, 'tp'), may hold values from -1 to 1
- value_branch: bfloat16 [1536, 1024], P('sp', 'tp'), may hold values from -6 to 6
- gate_branch: bfloat16 [1536, 1024], P('sp', 'tp'), may hold values from -6 to 6
Outputs:
- gradient_value: bfloat16 [1536, 1024], P('sp', 'tp')
- gradient_gating: bfloat16 [1536, 1024], P('sp', 'tp')
- gradient_mixer: float32 [2048, 1024], P('sp', 'tp')
- gradient_gate: float32 [8, 2048, 1024], P('sp', None, 'tp')
- gradient_up: float32 [8, 2048, 1024], P('sp', None, 'tp')
- gradient_down: float32 [8, 1024, 2048], P('sp', 'tp')
Inputs may be any that keep to these rules, and one draw needn't show every extreme that they name: `expert_ids`: the two experts of a token differ. Among the rows of one index of sp, at most 60 routes name the same expert, and in every draw some expert is named by exactly 60 of them.
All inputs are finite; a program needn't handle non-finite values.
Results may differ from a plain program's by a relative error of at most 0.012.
Values may be sent and summed in bfloat16 or wider, within the bound.
No kernel may reach another device: no remote copies, remote signals or barrier semaphores. Data moves between devices by JAX's collectives and lax.ppermute only.
A program may use at most 64 MiB of HBM per device.

v0:
```python
import jax
import jax.numpy as jnp
from jax import lax
from jax.sharding import PartitionSpec as P

EPS = 1e-06


def shifted(block, axis, distance):
    devices = range(lax.axis_size(axis))
    route = [(i - distance, i) for i in devices if i - distance in devices]
    return lax.ppermute(block, axis, route)


def route_slots(routes, capacity, experts):
    flat = routes.reshape(-1)
    onehot = (flat[:, None] == jnp.arange(experts, dtype=jnp.int32)[None, :]).astype(jnp.int32)
    before = jnp.cumsum(onehot, axis=0) - onehot
    position = jnp.sum(before * onehot, axis=1)
    slots = flat * capacity + position
    total = flat.shape[0]
    source = (
        jnp.full((experts * capacity,), total, jnp.int32)
        .at[slots]
        .set(jnp.arange(total, dtype=jnp.int32))
    )
    return (slots, source)


def silu_slope(value, sigma):
    return sigma * (1.0 + value * (1.0 - sigma))


def pack_routes(normed, scaled, source, experts, capacity):
    total = scaled.shape[0]
    token_index = jnp.where(source < total, source // 2, normed.shape[0])
    normed_ext = jnp.concatenate([normed, jnp.zeros((1, normed.shape[1]), normed.dtype)], axis=0)
    scaled_ext = jnp.concatenate([scaled, jnp.zeros((1, scaled.shape[1]), scaled.dtype)], axis=0)
    return (
        normed_ext[token_index].reshape(experts, capacity, -1),
        scaled_ext[source].reshape(experts, capacity, -1),
    )


def contract_last(left, right):
    return lax.dot_general(
        left, right, (((1,), (1,)), ((), ())), preferred_element_type=jnp.float32
    )


def contract_first(left, right):
    return lax.dot_general(
        left, right, (((0,), (0,)), ((), ())), preferred_element_type=jnp.float32
    )


def body(
    stream,
    upstream,
    expert_gain,
    expert_ids,
    group_weight,
    pair_scores,
    gate_weight,
    up_weight,
    down_weight,
    mixer_weight,
    filtered,
    channel_gain,
    kernel_taps,
    value_branch,
    gate_branch,
):
    experts = lax.axis_size("sp")
    tokens_here, width = stream.shape
    capacity = max(2, 5 * tokens_here // (2 * experts))
    groups = lax.axis_size("tp")
    column = width // groups
    first_col = lax.axis_index("tp") * column
    stream_f = stream.astype(jnp.float32)
    inv_rms = lax.rsqrt(jnp.mean(stream_f * stream_f, axis=1, keepdims=True) + EPS)
    normed = (stream_f * inv_rms * expert_gain).astype(jnp.bfloat16)
    spread = pair_scores[:, 0] - pair_scores[:, 1]
    route_weight = group_weight[:, None] * jnp.stack(
        [jax.nn.sigmoid(spread), jax.nn.sigmoid(-spread)], axis=1
    )
    scaled = (
        (route_weight[:, :, None] * upstream.astype(jnp.float32)[:, None, :])
        .astype(jnp.bfloat16)
        .reshape(2 * tokens_here, width)
    )
    slots, source = route_slots(expert_ids, capacity, experts)
    normed_part = lax.dynamic_slice_in_dim(normed, first_col, column, 1)
    scaled_part = lax.dynamic_slice_in_dim(scaled, first_col, column, 1)
    send_rows, send_cots = pack_routes(normed_part, scaled_part, source, experts, capacity)
    got_rows, got_cots = (
        lax.all_to_all(send_rows, "sp", split_axis=0, concat_axis=0, tiled=True),
        lax.all_to_all(send_cots, "sp", split_axis=0, concat_axis=0, tiled=True),
    )
    got_rows, got_cots = (
        lax.all_gather(got_rows, "tp", axis=2, tiled=True),
        lax.all_gather(got_cots, "tp", axis=2, tiled=True),
    )
    rows = got_rows.reshape(experts * capacity, width)
    cots = got_cots.reshape(experts * capacity, width)
    gate_local = gate_weight[0]
    up_local = up_weight[0]
    down_local = down_weight[0]
    pre_gate = jnp.dot(rows, gate_local, preferred_element_type=jnp.float32)
    pre_up = jnp.dot(rows, up_local, preferred_element_type=jnp.float32)
    sigma = jax.nn.sigmoid(pre_gate)
    silu_gate = pre_gate * sigma
    hidden = (silu_gate * pre_up).astype(jnp.bfloat16)
    grad_hidden = contract_last(cots, down_local)
    grad_pre_gate = (grad_hidden * pre_up * silu_slope(pre_gate, sigma)).astype(jnp.bfloat16)
    grad_pre_up = (grad_hidden * silu_gate).astype(jnp.bfloat16)
    partial_rows = contract_last(grad_pre_gate, gate_local) + contract_last(grad_pre_up, up_local)
    shared = lax.psum_scatter(
        partial_rows.astype(jnp.bfloat16), "tp", scatter_dimension=1, tiled=True
    )
    back = lax.all_to_all(
        shared.reshape(experts, capacity, column), "sp", split_axis=0, concat_axis=0, tiled=True
    )
    back = lax.all_gather(back, "tp", axis=2, tiled=True)
    gradient_gate = contract_first(rows, grad_pre_gate)[None]
    gradient_up = contract_first(rows, grad_pre_up)[None]
    gradient_down = contract_first(hidden, cots)[None]
    back_flat = back.reshape(experts * capacity, width)
    per_route = back_flat[slots].astype(jnp.float32).reshape(tokens_here, 2, width)
    grad_normed = per_route[:, 0] + per_route[:, 1]
    weighted = grad_normed * expert_gain
    inner = jnp.mean(weighted * stream_f, axis=1, keepdims=True)
    grad_stream = (
        upstream.astype(jnp.float32)
        + inv_rms * weighted
        - stream_f * inv_rms * inv_rms * inv_rms * inner
    ).astype(jnp.bfloat16)
    grad_act = contract_last(grad_stream, mixer_weight)
    filt = filtered.astype(jnp.float32)
    channels = filt.shape[1] * groups
    total_sum, total_square = lax.psum((jnp.sum(filt, axis=1), jnp.sum(filt * filt, axis=1)), "tp")
    mean_c = total_sum[:, None] / channels
    variance = total_square[:, None] / channels - mean_c * mean_c
    inv_std = lax.rsqrt(variance + EPS)
    centred = (filt - mean_c) * inv_std
    normal_out = centred * channel_gain
    sig_norm = jax.nn.sigmoid(normal_out)
    activated = (normal_out * sig_norm).astype(jnp.bfloat16)
    grad_centred = grad_act * silu_slope(normal_out, sig_norm) * channel_gain
    slope_sum, slope_cross = lax.psum(
        (jnp.sum(grad_centred, axis=1), jnp.sum(grad_centred * centred, axis=1)), "tp"
    )
    grad_filtered = (
        inv_std
        * (grad_centred - slope_sum[:, None] / channels - centred * slope_cross[:, None] / channels)
    ).astype(jnp.bfloat16)
    reach = kernel_taps.shape[0] - 1
    ahead = shifted(grad_filtered[:reach], "sp", -1)
    extended = jnp.concatenate([grad_filtered, ahead], axis=0).astype(jnp.float32)
    grad_mixed = lax.conv_general_dilated(
        extended[None],
        kernel_taps[::-1][:, None, :],
        (1,),
        "VALID",
        dimension_numbers=("NWC", "WIO", "NWC"),
        feature_group_count=filt.shape[1],
        precision=lax.Precision.HIGHEST,
    )[0]
    sig_gate = jax.nn.sigmoid(gate_branch.astype(jnp.float32))
    gradient_value = (grad_mixed * sig_gate).astype(jnp.bfloat16)
    gradient_gating = (
        grad_mixed * value_branch.astype(jnp.float32) * sig_gate * (1.0 - sig_gate)
    ).astype(jnp.bfloat16)
    gradient_mixer = lax.psum_scatter(
        contract_first(grad_stream, activated), "sp", scatter_dimension=0, tiled=True
    )
    return (
        gradient_value,
        gradient_gating,
        gradient_mixer,
        gradient_gate,
        gradient_up,
        gradient_down,
    )


def solution(mesh):
    return jax.shard_map(
        body,
        mesh=mesh,
        in_specs=(
            P("sp", None),
            P("sp", None),
            P(),
            P("sp", None),
            P("sp"),
            P("sp", None),
            P("sp", None, "tp"),
            P("sp", None, "tp"),
            P("sp", "tp", None),
            P("tp", None),
            P("sp", "tp"),
            P("tp"),
            P(None, "tp"),
            P("sp", "tp"),
            P("sp", "tp"),
        ),
        out_specs=(
            P("sp", "tp"),
            P("sp", "tp"),
            P("sp", "tp"),
            P("sp", None, "tp"),
            P("sp", None, "tp"),
            P("sp", "tp", None),
        ),
        check_vma=False,
    )
```

profile of v0, /device:TPU:0, one launch (start us, length us, event | category | flops | bytes accessed | tf_op | source)
XLA Modules:
  0.0 268.8 jit_solution(1533650336860865618)
XLA Ops:
  9.1 1.4 fusion
  10.5 1.3 convert_multiply_fusion.1
  13.3 2.9 %scatter_custom_fusion = s32[480]{0:T(512)S(1)} fusion(s32[384]{0:T(512)S(1)} %fusion.56, s32[384]{0:T(512)S(1)} %iota.11, s32[]{:T(128)} %constant.56.clone.1), kind=kCustom, calls=%fused_computation.99 | custom fusion | bytes 1924 | tf_op jit(solution)/shard_map/scatter | solution.py:25
  16.4 2.1 gather_fusion.1
  18.7 21.9 %all_to_all.15 = bf16[8,60,512]{2,1,0:T(8,128)(2,1)} all-to-all(bf16[8,60,512]{2,1,0:T(8,128)(2,1)S(1)} %reshape.138), channel_id=1, replica_groups=mesh['sp'=8,'tp'=4] {'sp'}, dimensions={0} | all-to-all | bytes 983040 | tf_op jit(solution)/shard_map/all_to_all | solution.py:97
  41.2 3.2 %mul.210 = f32[192,2,2048]{2,1,0:T(2,128)} broadcast(bf16[192,2048]{1,0:T(8,128)(2,1)S(1)} %copy-done.4), dimensions={0,2} | broadcast | bytes 3932160 | tf_op jit(solution)/shard_map/mul | solution.py:88
  44.5 5.6 %mul.211 = f32[384,2048]{1,0:T(8,128)} reshape(f32[192,2,2048]{2,1,0:T(2,128)} %mul.210) | data formatting | bytes 6291456 | tf_op jit(solution)/shard_map/mul | solution.py:88
  51.4 2.1 gather_fusion
  53.6 17.4 %all_to_all.16 = bf16[8,60,512]{2,1,0:T(8,128)(2,1)} all-to-all(bf16[8,60,512]{2,1,0:T(8,128)(2,1)S(1)} %reshape.136), channel_id=1, replica_groups=mesh['sp'=8,'tp'=4] {'sp'}, dimensions={0} | all-to-all | bytes 983040 | tf_op jit(solution)/shard_map/all_to_all | solution.py:98
  71.0 1.7 reshape.139
  72.8 2.6 fusion.10
  75.4 1.5 fusion.7
  76.9 15.8 %all-gather.4.cloned.1.call-done = bf16[8,60,2048]{2,1,0:T(8,128)(2,1)} async-done(((bf16[8,60,512]{2,1,0:T(8,128)(2,1)}), bf16[8,60,2048]{2,1,0:T(8,128)(2,1)}) %all-gather.4.cloned.1.call-update) | async-done | bytes 1966096 | tf_op jit(solution)/shard_map/all_gather | solution.py:102
  92.7 1.7 reshape.137
  94.5 2.8 %multiply_convert_fusion.1 = (bf16[480,256]{1,0:T(8,128)(2,1)S(1)}, bf16[480,256]{1,0:T(8,128)(2,1)S(1)}) fusion(f32[480,256]{1,0:T(8,128)} %fusion.7, f32[480,256]{1,0:T(8,128)S(1)} %fusion.10, bf16[480,2048]{1,0:T(8,128)(2,1)S(1)} %reshape.137, bf16[1,256,2048]{2,1,0:T(8,128)(2,1)} %param.23), kind=kOutput, calls=%fused_computation.31 | convolution fusion | flops 504913920 | bytes 4489216 | tf_op jit(solution)/shard_map/dot_general | solution.py:46
  98.8 2.0 add_convert_fusion
  100.8 30.5 %reduce-scatter.3.cloned.1.call-done = bf16[480,512]{1,0:T(8,128)(2,1)} async-done(((bf16[480,2048]{1,0:T(8,128)(2,1)}), bf16[480,512]{1,0:T(8,128)(2,1)}) %reduce-scatter.3.cloned.1.call-update) | async-done | bytes 491536 | tf_op jit(solution)/shard_map/reduce_scatter | solution.py:118
  132.4 19.8 %all_to_all.17 = bf16[8,60,512]{2,1,0:T(8,128)(2,1)} all-to-all(bf16[8,60,512]{2,1,0:T(8,128)(2,1)S(1)} %reshape.140), channel_id=1, replica_groups=mesh['sp'=8,'tp'=4] {'sp'}, dimensions={0} | all-to-all | bytes 983040 | tf_op jit(solution)/shard_map/all_to_all | solution.py:121
  152.5 6.1 %all-reduce.3 = (f32[192]{0:T(256)S(1)}, f32[192]{0:T(256)S(1)}) all-reduce(f32[192]{0:T(256)S(1)} %get-tuple-element.9, f32[192]{0:T(256)S(1)} %get-tuple-element.8), channel_id=1, replica_groups=mesh['sp'=8,'tp'=4] {'tp'}, use_global_device_ids=true, to_apply=%region_3.4 | all-reduce | flops 384 | bytes 3072 | tf_op jit(solution)/shard_map/psum | solution.py:141
  158.6 14.4 %all-gather.8.cloned.1.call-done = bf16[8,60,2048]{2,1,0:T(8,128)(2,1)} async-done(((bf16[8,60,512]{2,1,0:T(8,128)(2,1)}), bf16[8,60,2048]{2,1,0:T(8,128)(2,1)}) %all-gather.8.cloned.1.call-update) | async-done | bytes 1966096 | tf_op jit(solution)/shard_map/all_gather | solution.py:124
  173.0 1.7 reshape.141
  174.8 3.1 %gather_fusion.2 = bf16[384,2048]{1,0:T(8,128)(2,1)} fusion(bf16[480,2048]{1,0:T(8,128)(2,1)S(1)} %reshape.141, s32[1024]{0:T(1024)S(1)} %pad_clamp_fusion), kind=kCustom, calls=%fused_computation.2 | custom fusion | bytes 3147264 | tf_op jit(solution)/shard_map/gather | solution.py:129
  177.9 4.7 %reshape.142 = f32[192,2,2048]{2,1,0:T(2,128)} reshape(bf16[384,2048]{1,0:T(8,128)(2,1)} %gather_fusion.2) | data formatting | bytes 4718592 | tf_op jit(solution)/shard_map/convert_element_type | solution.py:129
  182.6 6.1 %fusion.62 = (f32[192,1,2048]{2,1,0:T(1,128)S(1)}, f32[192,1,2048]{2,1,0:T(1,128)S(1)}) fusion(f32[192,2,2048]{2,1,0:T(2,128)} %reshape.142), kind=kLoop, calls=%fused_computation.112 | loop fusion | bytes 6291456 | tf_op jit(solution)/shard_map/slice | solution.py:130
  189.9 1.9 subtract_convert_fusion
  191.8 1.9 fusion.42
  193.9 3.8 %convolution_bitcast_fusion.1 = f32[1,2048,256]{2,1,0:T(8,128)} fusion(bf16[480,2048]{1,0:T(8,128)(2,1)} %copy-done.6, bf16[480,256]{1,0:T(8,128)(2,1)S(1)} %copy-done.13), kind=kOutput, calls=%fused_computation.6 | convolution fusion | flops 503316480 | bytes 4308992 | tf_op jit(solution)/shard_map/dot_general | solution.py:52
  197.7 2.1 convolution_bitcast_fusion
  200.5 6.3 %all-reduce.2 = (f32[192]{0:T(256)S(1)}, f32[192]{0:T(256)S(1)}) all-reduce(f32[192]{0:T(256)S(1)} %get-tuple-element.7, f32[192]{0:T(256)S(1)} %get-tuple-element.6), channel_id=1, replica_groups=mesh['sp'=8,'tp'=4] {'tp'}, use_global_device_ids=true, to_apply=%region_14.15 | all-reduce | flops 384 | bytes 3072 | tf_op jit(solution)/shard_map/psum | solution.py:150
  208.3 3.6 %convolution_bitcast_fusion.2 = f32[1,2048,256]{2,1,0:T(8,128)} fusion(bf16[480,2048]{1,0:T(8,128)(2,1)} %copy-done.6, bf16[480,256]{1,0:T(8,128)(2,1)S(1)} %copy-done.15), kind=kOutput, calls=%fused_computation.7 | convolution fusion | flops 503316480 | bytes 4308992 | tf_op jit(solution)/shard_map/dot_general | solution.py:52
  212.6 2.9 %fusion.17 = f32[1,192,256]{2,0,1:T(1,128)S(1)} fusion(bf16[1,222,256]{2,1,0:T(8,128)(2,1)S(1)} %maximum_bitcast_fusion, f32[31,1,256]{2,0,1:T(8,128)S(1)} %bitcast.71), kind=kOutput, calls=%fused_computation.40 | convolution fusion | flops 18284544 | bytes 342016 | tf_op jit(solution)/shard_map/conv_general_dilated | solution.py:160
  216.2 46.0 %reduce-scatter.5.cloned.1.call-done = f32[256,256]{1,0:T(8,128)} async-done(((f32[2048,256]{1,0:T(8,128)}), f32[256,256]{1,0:T(8,128)}) %reduce-scatter.5.cloned.1.call-update) | async-done | bytes 262160 | tf_op jit(solution)/shard_map/reduce_scatter | solution.py:174
  (106 shorter events, 13.3 us)
Async XLA Ops:
  7.2 68.3 %copy-start = (bf16[1,2048,256]{2,1,0:T(8,128)(2,1)S(1)}, bf16[1,2048,256]{2,1,0:T(8,128)(2,1)}, u32[]{:S(2)}) copy-start(bf16[1,2048,256]{2,1,0:T(8,128)(2,1)} %param.21) | copy-start | bytes 3145732
  7.2 9.1 %copy-start.18 = (f32[2048]{0:T(1024)S(1)}, f32[2048]{0:T(1024)}, u32[]{:S(2)}) copy-start(f32[2048]{0:T(1024)} %param.17) | copy-start | bytes 24580
  7.2 63.8 %all-gather.6.cloned.1.call-start = ((), (), s32[]{:S(2)}) async-start(), calls=%async_computation.6 | async-start | bytes 2621440 | tf_op jit(solution)/shard_map/all_gather | solution.py:101
  18.6 22.1 %copy-start.20 = (f32[192,2]{0,1:T(2,128)S(1)}, f32[192,2]{0,1:T(2,128)}, u32[]{:S(2)}) copy-start(f32[192,2]{0,1:T(2,128)} %param.20) | copy-start | bytes 4612
  18.6 22.4 %copy-start.21 = (f32[192]{0:T(256)S(1)}, f32[192]{0:T(256)}, u32[]{:S(2)}) copy-start(f32[192]{0:T(256)} %param.19) | copy-start | bytes 2308
  18.6 22.6 %copy-start.4 = (bf16[192,2048]{1,0:T(8,128)(2,1)S(1)}, bf16[192,2048]{1,0:T(8,128)(2,1)}, u32[]{:S(2)}) copy-start(bf16[192,2048]{1,0:T(8,128)(2,1)} %param.16) | copy-start | bytes 2359300
  40.6 52.1 %all-gather.4.cloned.1.call-start = ((), (), s32[]{:S(2)}) async-start(), calls=%async_computation.5 | async-start | bytes 2621440 | tf_op jit(solution)/shard_map/all_gather | solution.py:102
  71.0 60.4 %reduce-scatter.3.cloned.1.call-start = ((), (), s32[]{:S(2)}) async-start(), calls=%async_computation.7 | async-start | bytes 2457600 | tf_op jit(solution)/shard_map/reduce_scatter | solution.py:118
  72.8 4.1 %copy-start.6 = (bf16[480,2048]{1,0:T(8,128)(2,1)}, bf16[480,2048]{1,0:T(8,128)(2,1)S(1)}, u32[]{:S(2)}) copy-start(bf16[480,2048]{1,0:T(8,128)(2,1)S(1)} %reshape.139) | copy-start | bytes 5898244
  75.4 19.1 %copy-start.9 = (f32[480,256]{1,0:T(8,128)}, f32[480,256]{1,0:T(8,128)S(1)}, u32[]{:S(2)}) copy-start(f32[480,256]{1,0:T(8,128)S(1)} %fusion.10) | copy-start | bytes 1474564
  94.5 2.8 %copy-start.2 = (bf16[480,2048]{1,0:T(8,128)(2,1)}, bf16[480,2048]{1,0:T(8,128)(2,1)S(1)}, u32[]{:S(2)}) copy-start(bf16[480,2048]{1,0:T(8,128)(2,1)S(1)} %reshape.137) | copy-start | bytes 5898244
  97.4 0.8 copy-start.14
  97.4 0.8 copy-start.12
  97.4 1.4 copy-start.7
  100.8 51.5 %copy-start.8 = (bf16[192,256]{1,0:T(8,128)(2,1)S(1)}, bf16[192,256]{1,0:T(8,128)(2,1)}, u32[]{:S(2)}) copy-start(bf16[192,256]{1,0:T(8,128)(2,1)} %param.25) | copy-start | bytes 294916
  100.8 72.3 %all-gather.8.cloned.1.call-start = ((), (), s32[]{:S(2)}) async-start(), calls=%async_computation.8 | async-start | bytes 2621440 | tf_op jit(solution)/shard_map/all_gather | solution.py:124
  152.3 110.0 %reduce-scatter.5.cloned.1.call-start = ((), (), s32[]{:S(2)}) async-start(), calls=%async_computation.9 | async-start | bytes 2359296 | tf_op jit(solution)/shard_map/reduce_scatter | solution.py:174
  182.6 6.1 %copy-start.1 = (bf16[192,2048]{1,0:T(8,128)(2,1)S(1)}, bf16[192,2048]{1,0:T(8,128)(2,1)}, u32[]{:S(2)}) copy-start(bf16[192,2048]{1,0:T(8,128)(2,1)} %param.15) | copy-start | bytes 2359300
  188.8 1.1 copy-start.5
  189.9 1.9 copy-start.22
  191.8 1.9 copy-start.19
  191.8 2.0 copy-start.13
  193.9 3.8 %copy-start.3 = (bf16[480,2048]{1,0:T(8,128)(2,1)S(1)}, bf16[480,2048]{1,0:T(8,128)(2,1)}, u32[]{:S(2)}) copy-start(bf16[480,2048]{1,0:T(8,128)(2,1)} %copy-done.2) | copy-start | bytes 5898244
  193.9 3.8 %copy-start.10 = (f32[480,256]{1,0:T(8,128)S(1)}, f32[480,256]{1,0:T(8,128)}, u32[]{:S(2)}) copy-start(f32[480,256]{1,0:T(8,128)} %copy-done.9) | copy-start | bytes 1474564
  193.9 3.8 %copy-start.11 = (f32[480,256]{1,0:T(8,128)S(1)}, f32[480,256]{1,0:T(8,128)}, u32[]{:S(2)}) copy-start(f32[480,256]{1,0:T(8,128)} %fusion.7) | copy-start | bytes 1474564
  197.7 2.1 copy-start.23
  199.8 8.4 %copy-start.15 = (bf16[480,256]{1,0:T(8,128)(2,1)S(1)}, bf16[480,256]{1,0:T(8,128)(2,1)}, u32[]{:S(2)}) copy-start(bf16[480,256]{1,0:T(8,128)(2,1)} %copy-done.14) | copy-start | bytes 737284
  206.9 5.6 %collective-permute-start = (bf16[30,256]{1,0:T(8,128)(2,1)S(1)}, bf16[30,256]{1,0:T(8,128)(2,1)S(1)}, u32[]{:S(2)}, u32[]{:S(2)}) collective-permute-start(bf16[30,256]{1,0:T(8,128)(2,1)S(1)} %slice.37), channel_id=1, source_target_pairs={{4,0},{8,4},{12,8},{16,12},{20,16},{24,20},{28,24},{5,1},{9,5},{13... | collective-permute-start | bytes 46088 | tf_op jit(solution)/shard_map/ppermute | solution.py:12
  212.6 2.9 %copy-start.16 = (bf16[192,256]{1,0:T(8,128)(2,1)S(1)}, bf16[192,256]{1,0:T(8,128)(2,1)}, u32[]{:S(2)}) copy-start(bf16[192,256]{1,0:T(8,128)(2,1)} %param.28) | copy-start | bytes 294916
  212.6 2.9 %copy-start.17 = (bf16[192,256]{1,0:T(8,128)(2,1)S(1)}, bf16[192,256]{1,0:T(8,128)(2,1)}, u32[]{:S(2)}) copy-start(bf16[192,256]{1,0:T(8,128)(2,1)} %param.29) | copy-start | bytes 294916
Sparse Core Ops, SparseCore 0:
  40.7 21.5 all-gather.5
  71.1 21.6 all-gather.3
  100.9 30.3 reduce-scatter.2
  152.4 20.6 all-gather.7
  193.9 68.3 reduce-scatter.4
where the time goes:
time: 270 us; the launch traced here: 269 us
  waiting for transfers between devices  108 us (40%)
  blocking collectives  71.4 us (26%)
  local copies, waits for them, and re-layouts  39.8 us (15%)
  matrix products  24.5 us (9%)
  between operations  14.4 us (5%)
  other arithmetic  9.69 us (4%)
    reduce_scatter x1, waiting for transfers between devices, body(): lax.psum_scatter(contract_first(grad_stream, activated), 'sp', scatter_di...  46 us
    reduce_scatter x1, waiting for transfers between devices, body(): lax.psum_scatter(partial_rows.astype(jnp.bfloat16), 'tp', scatter_dimensi...  30.5 us
    all_to_all x1, blocking collectives, body(): lax.all_to_all(send_rows, 'sp', split_axis=0, concat_axis=0, tiled=True)  21.9 us
    all_to_all x1, blocking collectives, body(): lax.all_to_all(shared.reshape(experts, capacity, column), 'sp', split_axi...  19.8 us
    all_to_all x1, blocking collectives, body(): lax.all_to_all(send_cots, 'sp', split_axis=0, concat_axis=0, tiled=True)  17.4 us
    all_gather x1, waiting for transfers between devices, body(): lax.all_gather(got_cots, 'tp', axis=2, tiled=True)  15.8 us
    all_gather x1, waiting for transfers between devices, body(): back = lax.all_gather(back, 'tp', axis=2, tiled=True)  14.4 us
    dot_general x4, matrix products, contract_first(): lax.dot_general(left, right, (((0,), (0,)), ((), ())), preferred_element_...  11.4 us
  transfers between devices with their start and end apart: 6, of which 5 were waited for; matrix products, arithmetic and copies ran while one was open for 12% of the time, Pallas kernels for 0%

commit v1 on v0

--- a/solution.py
+++ b/solution.py
@@ -121,7 +121,12 @@
     back = lax.all_to_all(
         shared.reshape(experts, capacity, column), "sp", split_axis=0, concat_axis=0, tiled=True
     )
-    back = lax.all_gather(back, "tp", axis=2, tiled=True)
+    ring = [back]
+    for hop in range(3):
+        ring.append(lax.ppermute(ring[-1], "tp", [(dev, (dev + 1) % 4) for dev in range(4)]))
+    back = jnp.roll(
+        jnp.concatenate(ring[::-1], axis=2), (lax.axis_index("tp") + 1) * ring[0].shape[2], axis=2
+    )
     gradient_gate = contract_first(rows, grad_pre_gate)[None]
     gradient_up = contract_first(rows, grad_pre_up)[None]
     gradient_down = contract_first(hidden, cots)[None]

time: 270 us -> 276 us (1.022)
  blocking collectives: 71.4 us -> 74.5 us
    ppermute x0 -> x3, waiting for transfers between devices: none -> 17.2 us  [body(): lax.ppermute(ring[-1], 'tp', [(dev, (dev + 1) % 4) for dev in range(4)])]
    all_gather x1 -> x0, waiting for transfers between devices: 14.4 us -> none  [body(): back = lax.all_gather(back, 'tp', axis=2, tiled=True)]
    psum x1, blocking collectives: 6.12 us -> 9.38 us  [body(): lax.psum((jnp.sum(filt, axis=1), jnp.sum(filt * filt, axis=1)), 'tp')]
  transfers between devices with their start and end apart: 6 -> 8, of which waited for: 5 -> 6; matrix products, arithmetic and copies ran while one was open for 12% -> 12% of each run, Pallas kernels for 0% -> 0%
where the time goes in v1:
time: 276 us; the launch traced here: 275 us
  waiting for transfers between devices  108 us (39%)
  blocking collectives  74.5 us (27%)
  local copies, waits for them, and re-layouts  41.9 us (15%)
  matrix products  24.5 us (9%)
  between operations  14.4 us (5%)
  other arithmetic  9.69 us (4%)
    reduce_scatter x1, waiting for transfers between devices, body(): lax.psum_scatter(contract_first(grad_stream, activated), 'sp', scatter_di...  44 us
    reduce_scatter x1, waiting for transfers between devices, body(): lax.psum_scatter(partial_rows.astype(jnp.bfloat16), 'tp', scatter_dimensi...  30.5 us
    all_to_all x1, blocking collectives, body(): lax.all_to_all(send_rows, 'sp', split_axis=0, concat_axis=0, tiled=True)  21.9 us
    all_to_all x1, blocking collectives, body(): lax.all_to_all(shared.reshape(experts, capacity, column), 'sp', split_axi...  19.7 us
    all_to_all x1, blocking collectives, body(): lax.all_to_all(send_cots, 'sp', split_axis=0, concat_axis=0, tiled=True)  17.4 us
    ppermute x3, waiting for transfers between devices, body(): lax.ppermute(ring[-1], 'tp', [(dev, (dev + 1) % 4) for dev in range(4)])  17.2 us
    all_gather x1, waiting for transfers between devices, body(): lax.all_gather(got_cots, 'tp', axis=2, tiled=True)  15.8 us
    dot_general x4, matrix products, contract_first(): lax.dot_general(left, right, (((0,), (0,)), ((), ())), preferred_element_...  11.5 us
  transfers between devices with their start and end apart: 8, of which 6 were waited for; matrix products, arithmetic and copies ran while one was open for 12% of the time, Pallas kernels for 0%

profile of v1, /device:TPU:0, one launch (start us, length us, event | category | flops | bytes accessed | tf_op | source)
XLA Modules:
  0.0 274.9 jit_solution(9423651058188426807)
XLA Ops:
  13.3 2.9 %scatter_custom_fusion = s32[480]{0:T(512)S(1)} fusion(s32[384]{0:T(512)S(1)} %fusion.56, s32[384]{0:T(512)S(1)} %iota.11, s32[]{:T(128)} %constant.75.clone.1), kind=kCustom, calls=%fused_computation.107 | custom fusion | bytes 1924 | tf_op jit(solution)/shard_map/scatter | solution.py:25
  16.4 2.1 gather_fusion.1
  18.7 21.9 %all_to_all.15 = bf16[8,60,512]{2,1,0:T(8,128)(2,1)} all-to-all(bf16[8,60,512]{2,1,0:T(8,128)(2,1)S(1)} %reshape.138), channel_id=1, replica_groups=mesh['sp'=8,'tp'=4] {'sp'}, dimensions={0} | all-to-all | bytes 983040 | tf_op jit(solution)/shard_map/all_to_all | solution.py:97
  41.2 3.2 %mul.213 = f32[192,2,2048]{2,1,0:T(2,128)} broadcast(bf16[192,2048]{1,0:T(8,128)(2,1)S(1)} %copy-done.4), dimensions={0,2} | broadcast | bytes 3932160 | tf_op jit(solution)/shard_map/mul | solution.py:88
  44.5 5.6 %mul.214 = f32[384,2048]{1,0:T(8,128)} reshape(f32[192,2,2048]{2,1,0:T(2,128)} %mul.213) | data formatting | bytes 6291456 | tf_op jit(solution)/shard_map/mul | solution.py:88
  51.4 2.1 gather_fusion
  53.6 17.4 %all_to_all.16 = bf16[8,60,512]{2,1,0:T(8,128)(2,1)} all-to-all(bf16[8,60,512]{2,1,0:T(8,128)(2,1)S(1)} %reshape.136), channel_id=1, replica_groups=mesh['sp'=8,'tp'=4] {'sp'}, dimensions={0} | all-to-all | bytes 983040 | tf_op jit(solution)/shard_map/all_to_all | solution.py:98
  71.0 1.7 reshape.139
  72.8 2.6 fusion.10
  75.4 1.5 fusion.7
  76.9 15.8 %all-gather.3.cloned.1.call-done = bf16[8,60,2048]{2,1,0:T(8,128)(2,1)} async-done(((bf16[8,60,512]{2,1,0:T(8,128)(2,1)}), bf16[8,60,2048]{2,1,0:T(8,128)(2,1)}) %all-gather.3.cloned.1.call-update) | async-done | bytes 1966096 | tf_op jit(solution)/shard_map/all_gather | solution.py:102
  92.7 1.7 reshape.137
  94.5 2.8 %multiply_convert_fusion.1 = (bf16[480,256]{1,0:T(8,128)(2,1)S(1)}, bf16[480,256]{1,0:T(8,128)(2,1)S(1)}) fusion(f32[480,256]{1,0:T(8,128)} %fusion.7, f32[480,256]{1,0:T(8,128)S(1)} %fusion.10, bf16[480,2048]{1,0:T(8,128)(2,1)S(1)} %reshape.137, bf16[1,256,2048]{2,1,0:T(8,128)(2,1)} %param.23), kind=kOutput, calls=%fused_computation.31 | convolution fusion | flops 504913920 | bytes 4489216 | tf_op jit(solution)/shard_map/dot_general | solution.py:46
  98.8 2.0 add_convert_fusion
  100.8 30.5 %reduce-scatter.3.cloned.1.call-done = bf16[480,512]{1,0:T(8,128)(2,1)} async-done(((bf16[480,2048]{1,0:T(8,128)(2,1)}), bf16[480,512]{1,0:T(8,128)(2,1)}) %reduce-scatter.3.cloned.1.call-update) | async-done | bytes 491536 | tf_op jit(solution)/shard_map/reduce_scatter | solution.py:118
  132.4 19.7 %all_to_all.17 = bf16[8,60,512]{2,1,0:T(8,128)(2,1)S(1)} all-to-all(bf16[8,60,512]{2,1,0:T(8,128)(2,1)S(1)} %reshape.140), channel_id=1, replica_groups=mesh['sp'=8,'tp'=4] {'sp'}, dimensions={0} | all-to-all | bytes 983040 | tf_op jit(solution)/shard_map/all_to_all | solution.py:121
  152.1 8.6 %collective-permute-done = bf16[8,60,512]{2,1,0:T(8,128)(2,1)S(1)} collective-permute-done((bf16[8,60,512]{2,1,0:T(8,128)(2,1)S(1)}, bf16[8,60,512]{2,1,0:T(8,128)(2,1)S(1)}, u32[]{:S(2)}, u32[]{:S(2)}) %collective-permute-start) | collective-permute-done | bytes 491552 | tf_op jit(solution)/shard_map/ppermute | solution.py:126
  160.7 8.6 %collective-permute-done.1 = bf16[8,60,512]{2,1,0:T(8,128)(2,1)S(1)} collective-permute-done((bf16[8,60,512]{2,1,0:T(8,128)(2,1)S(1)}, bf16[8,60,512]{2,1,0:T(8,128)(2,1)S(1)}, u32[]{:S(2)}, u32[]{:S(2)}) %collective-permute-start.1) | collective-permute-done | bytes 491552 | tf_op jit(solution)/shard_map/ppermute | solution.py:126
  169.5 9.4 %all-reduce.3 = (f32[192]{0:T(256)S(1)}, f32[192]{0:T(256)S(1)}) all-reduce(f32[192]{0:T(256)S(1)} %get-tuple-element.9, f32[192]{0:T(256)S(1)} %get-tuple-element.8), channel_id=1, replica_groups=mesh['sp'=8,'tp'=4] {'tp'}, use_global_device_ids=true, to_apply=%region_3.4 | all-reduce | flops 384 | bytes 3072 | tf_op jit(solution)/shard_map/psum | solution.py:146
  179.5 1.6 constant_dynamic-slice_fusion
  181.1 1.7 reshape.141
  182.8 3.1 %gather_fusion.2 = bf16[384,2048]{1,0:T(8,128)(2,1)} fusion(bf16[480,2048]{1,0:T(8,128)(2,1)S(1)} %reshape.141, s32[1024]{0:T(1024)S(1)} %pad_clamp_fusion), kind=kCustom, calls=%fused_computation.2 | custom fusion | bytes 3147264 | tf_op jit(solution)/shard_map/gather | solution.py:134
  186.0 4.7 %reshape.142 = f32[192,2,2048]{2,1,0:T(2,128)} reshape(bf16[384,2048]{1,0:T(8,128)(2,1)} %gather_fusion.2) | data formatting | bytes 4718592 | tf_op jit(solution)/shard_map/convert_element_type | solution.py:134
  190.7 6.1 %fusion.62 = (f32[192,1,2048]{2,1,0:T(1,128)S(1)}, f32[192,1,2048]{2,1,0:T(1,128)S(1)}) fusion(f32[192,2,2048]{2,1,0:T(2,128)} %reshape.142), kind=kLoop, calls=%fused_computation.121 | loop fusion | bytes 6291456 | tf_op jit(solution)/shard_map/slice | solution.py:135
  198.0 1.9 subtract_convert_fusion
  199.9 1.9 fusion.42
  202.0 3.8 %convolution_bitcast_fusion.1 = f32[1,2048,256]{2,1,0:T(8,128)} fusion(bf16[480,2048]{1,0:T(8,128)(2,1)} %copy-done.6, bf16[480,256]{1,0:T(8,128)(2,1)S(1)} %copy-done.13), kind=kOutput, calls=%fused_computation.6 | convolution fusion | flops 503316480 | bytes 4308992 | tf_op jit(solution)/shard_map/dot_general | solution.py:52
  205.8 2.1 convolution_bitcast_fusion
  208.5 6.2 %all-reduce.2 = (f32[192]{0:T(256)S(1)}, f32[192]{0:T(256)S(1)}) all-reduce(f32[192]{0:T(256)S(1)} %get-tuple-element.7, f32[192]{0:T(256)S(1)} %get-tuple-element.6), channel_id=1, replica_groups=mesh['sp'=8,'tp'=4] {'tp'}, use_global_device_ids=true, to_apply=%region_14.15 | all-reduce | flops 384 | bytes 3072 | tf_op jit(solution)/shard_map/psum | solution.py:155
  216.3 3.7 %convolution_bitcast_fusion.2 = f32[1,2048,256]{2,1,0:T(8,128)} fusion(bf16[480,2048]{1,0:T(8,128)(2,1)} %copy-done.6, bf16[480,256]{1,0:T(8,128)(2,1)S(1)} %copy-done.15), kind=kOutput, calls=%fused_computation.7 | convolution fusion | flops 503316480 | bytes 4308992 | tf_op jit(solution)/shard_map/dot_general | solution.py:52
  220.8 2.9 %fusion.17 = f32[1,192,256]{2,0,1:T(1,128)S(1)} fusion(bf16[1,222,256]{2,1,0:T(8,128)(2,1)S(1)} %maximum_bitcast_fusion, f32[31,1,256]{2,0,1:T(8,128)S(1)} %bitcast.71), kind=kOutput, calls=%fused_computation.40 | convolution fusion | flops 18284544 | bytes 342016 | tf_op jit(solution)/shard_map/conv_general_dilated | solution.py:165
  224.4 44.0 %reduce-scatter.5.cloned.1.call-done = f32[256,256]{1,0:T(8,128)} async-done(((f32[2048,256]{1,0:T(8,128)}), f32[256,256]{1,0:T(8,128)}) %reduce-scatter.5.cloned.1.call-update) | async-done | bytes 262160 | tf_op jit(solution)/shard_map/reduce_scatter | solution.py:179
  (118 shorter events, 16.6 us)
Async XLA Ops:
  7.2 68.3 %copy-start = (bf16[1,2048,256]{2,1,0:T(8,128)(2,1)S(1)}, bf16[1,2048,256]{2,1,0:T(8,128)(2,1)}, u32[]{:S(2)}) copy-start(bf16[1,2048,256]{2,1,0:T(8,128)(2,1)} %param.21) | copy-start | bytes 3145732
  7.2 9.1 %copy-start.18 = (f32[2048]{0:T(1024)S(1)}, f32[2048]{0:T(1024)}, u32[]{:S(2)}) copy-start(f32[2048]{0:T(1024)} %param.17) | copy-start | bytes 24580
  7.2 63.8 %all-gather.5.cloned.1.call-start = ((), (), s32[]{:S(2)}) async-start(), calls=%async_computation.6 | async-start | bytes 2621440 | tf_op jit(solution)/shard_map/all_gather | solution.py:101
  18.6 22.1 %copy-start.20 = (f32[192,2]{0,1:T(2,128)S(1)}, f32[192,2]{0,1:T(2,128)}, u32[]{:S(2)}) copy-start(f32[192,2]{0,1:T(2,128)} %param.20) | copy-start | bytes 4612
  18.6 22.4 %copy-start.21 = (f32[192]{0:T(256)S(1)}, f32[192]{0:T(256)}, u32[]{:S(2)}) copy-start(f32[192]{0:T(256)} %param.19) | copy-start | bytes 2308
  18.6 22.6 %copy-start.4 = (bf16[192,2048]{1,0:T(8,128)(2,1)S(1)}, bf16[192,2048]{1,0:T(8,128)(2,1)}, u32[]{:S(2)}) copy-start(bf16[192,2048]{1,0:T(8,128)(2,1)} %param.16) | copy-start | bytes 2359300
  40.6 52.1 %all-gather.3.cloned.1.call-start = ((), (), s32[]{:S(2)}) async-start(), calls=%async_computation.5 | async-start | bytes 2621440 | tf_op jit(solution)/shard_map/all_gather | solution.py:102
  71.0 60.4 %reduce-scatter.3.cloned.1.call-start = ((), (), s32[]{:S(2)}) async-start(), calls=%async_computation.7 | async-start | bytes 2457600 | tf_op jit(solution)/shard_map/reduce_scatter | solution.py:118
  72.8 4.1 %copy-start.6 = (bf16[480,2048]{1,0:T(8,128)(2,1)}, bf16[480,2048]{1,0:T(8,128)(2,1)S(1)}, u32[]{:S(2)}) copy-start(bf16[480,2048]{1,0:T(8,128)(2,1)S(1)} %reshape.139) | copy-start | bytes 5898244
  75.4 19.1 %copy-start.9 = (f32[480,256]{1,0:T(8,128)}, f32[480,256]{1,0:T(8,128)S(1)}, u32[]{:S(2)}) copy-start(f32[480,256]{1,0:T(8,128)S(1)} %fusion.10) | copy-start | bytes 1474564
  94.5 2.8 %copy-start.2 = (bf16[480,2048]{1,0:T(8,128)(2,1)}, bf16[480,2048]{1,0:T(8,128)(2,1)S(1)}, u32[]{:S(2)}) copy-start(bf16[480,2048]{1,0:T(8,128)(2,1)S(1)} %reshape.137) | copy-start | bytes 5898244
  97.4 0.8 copy-start.14
  97.4 0.8 copy-start.12
  97.4 1.4 copy-start.7
  100.8 68.6 %copy-start.8 = (bf16[192,256]{1,0:T(8,128)(2,1)S(1)}, bf16[192,256]{1,0:T(8,128)(2,1)}, u32[]{:S(2)}) copy-start(bf16[192,256]{1,0:T(8,128)(2,1)} %param.25) | copy-start | bytes 294916
  100.8 167.6 %reduce-scatter.5.cloned.1.call-start = ((), (), s32[]{:S(2)}) async-start(), calls=%async_computation.8 | async-start | bytes 2359296 | tf_op jit(solution)/shard_map/reduce_scatter | solution.py:179
  152.1 8.6 %collective-permute-start = (bf16[8,60,512]{2,1,0:T(8,128)(2,1)S(1)}, bf16[8,60,512]{2,1,0:T(8,128)(2,1)S(1)}, u32[]{:S(2)}, u32[]{:S(2)}) collective-permute-start(bf16[8,60,512]{2,1,0:T(8,128)(2,1)S(1)} %all_to_all.17), channel_id=1, source_target_pairs={{0,1},{1,2},{2,3},{3,0},{4,5},{5,6},{6,7},{7,4},{8,9},{9,10},{10,1... | collective-permute-start | bytes 1474568 | tf_op jit(solution)/shard_map/ppermute | solution.py:126
  160.7 8.6 %collective-permute-start.1 = (bf16[8,60,512]{2,1,0:T(8,128)(2,1)S(1)}, bf16[8,60,512]{2,1,0:T(8,128)(2,1)S(1)}, u32[]{:S(2)}, u32[]{:S(2)}) collective-permute-start(bf16[8,60,512]{2,1,0:T(8,128)(2,1)S(1)} %collective-permute-done), channel_id=1, source_target_pairs={{0,1},{1,2},{2,3},{3,0},{4,5},{5,6},{6,7},{7,4},{8,9},{9,10},{10,1... | collective-permute-start | bytes 1474568 | tf_op jit(solution)/shard_map/ppermute | solution.py:126
  169.3 9.6 %collective-permute-start.2 = (bf16[8,60,512]{2,1,0:T(8,128)(2,1)S(1)}, bf16[8,60,512]{2,1,0:T(8,128)(2,1)S(1)}, u32[]{:S(2)}, u32[]{:S(2)}) collective-permute-start(bf16[8,60,512]{2,1,0:T(8,128)(2,1)S(1)} %collective-permute-done.1), channel_id=1, source_target_pairs={{0,1},{1,2},{2,3},{3,0},{4,5},{5,6},{6,7},{7,4},{8,9},{9,10},{10,1... | collective-permute-start | bytes 1474568 | tf_op jit(solution)/shard_map/ppermute | solution.py:126
  190.7 6.1 %copy-start.1 = (bf16[192,2048]{1,0:T(8,128)(2,1)S(1)}, bf16[192,2048]{1,0:T(8,128)(2,1)}, u32[]{:S(2)}) copy-start(bf16[192,2048]{1,0:T(8,128)(2,1)} %param.15) | copy-start | bytes 2359300
  196.8 1.1 copy-start.5
  198.0 1.9 copy-start.22
  199.9 2.0 copy-start.19
  199.9 2.0 copy-start.13
  201.9 3.8 %copy-start.3 = (bf16[480,2048]{1,0:T(8,128)(2,1)S(1)}, bf16[480,2048]{1,0:T(8,128)(2,1)}, u32[]{:S(2)}) copy-start(bf16[480,2048]{1,0:T(8,128)(2,1)} %copy-done.2) | copy-start | bytes 5898244
  201.9 3.8 %copy-start.10 = (f32[480,256]{1,0:T(8,128)S(1)}, f32[480,256]{1,0:T(8,128)}, u32[]{:S(2)}) copy-start(f32[480,256]{1,0:T(8,128)} %copy-done.9) | copy-start | bytes 1474564
  201.9 3.8 %copy-start.11 = (f32[480,256]{1,0:T(8,128)S(1)}, f32[480,256]{1,0:T(8,128)}, u32[]{:S(2)}) copy-start(f32[480,256]{1,0:T(8,128)} %fusion.7) | copy-start | bytes 1474564
  205.8 2.1 copy-start.23
  207.9 8.4 %copy-start.15 = (bf16[480,256]{1,0:T(8,128)(2,1)S(1)}, bf16[480,256]{1,0:T(8,128)(2,1)}, u32[]{:S(2)}) copy-start(bf16[480,256]{1,0:T(8,128)(2,1)} %copy-done.14) | copy-start | bytes 737284
  215.0 5.8 %collective-permute-start.3 = (bf16[30,256]{1,0:T(8,128)(2,1)S(1)}, bf16[30,256]{1,0:T(8,128)(2,1)S(1)}, u32[]{:S(2)}, u32[]{:S(2)}) collective-permute-start(bf16[30,256]{1,0:T(8,128)(2,1)S(1)} %slice.37), channel_id=1, source_target_pairs={{4,0},{8,4},{12,8},{16,12},{20,16},{24,20},{28,24},{5,1},{9,5},{13... | collective-permute-start | bytes 46088 | tf_op jit(solution)/shard_map/ppermute | solution.py:12
  220.7 2.9 %copy-start.16 = (bf16[192,256]{1,0:T(8,128)(2,1)S(1)}, bf16[192,256]{1,0:T(8,128)(2,1)}, u32[]{:S(2)}) copy-start(bf16[192,256]{1,0:T(8,128)(2,1)} %param.28) | copy-start | bytes 294916
  220.8 2.9 %copy-start.17 = (bf16[192,256]{1,0:T(8,128)(2,1)S(1)}, bf16[192,256]{1,0:T(8,128)(2,1)}, u32[]{:S(2)}) copy-start(bf16[192,256]{1,0:T(8,128)(2,1)} %param.29) | copy-start | bytes 294916
Sparse Core Ops, SparseCore 0:
  40.7 21.5 all-gather.4
  71.1 21.6 all-gather.2
  100.9 30.3 reduce-scatter.2
  201.9 66.4 reduce-scatter.4
